TPU v7x, 128 devices: a whole 4x4x4 slice. The times are simulated.
128 devices in a mesh: sp: 32 (over z, y, core), tp: 4 (over x).
Axes of the slice: x: 4, y: 4, z: 4, core: 2. Of those that a mesh axis runs over, the one named last changes fastest.
Arguments:
- queries: bfloat16 [32768, 1024], P('sp', 'tp'), may hold values from -8 to 8
- keys: bfloat16 [32768, 256], P('sp', 'tp'), may hold values from -8 to 8
- values: bfloat16 [32768, 256], P('sp', 'tp'), may hold values from -18 to 18
- doc_ids: int32 [32768], P('sp'), may hold values from 0 to 7, never falling along the last dimension, each value on 1 to 16384 neighbouring positions
- sinks: float32 [16], P('tp'), may hold values from 0 to 4
- residual: bfloat16 [32768, 2048], P(('sp', 'tp')), may hold values from -12 to 12
- out_weight: bfloat16 [1024, 2048], P('tp'), may hold values from -0.1875 to 0.1875
- norm_gain: float32 [2048], replicated, may hold values from 0.1 to 1.9
- w_gate: bfloat16 [2048, 5632], P('sp', 'tp'), may hold values from -0.125 to 0.125
- w_value: bfloat16 [2048, 5632], P('sp', 'tp'), may hold values from -0.125 to 0.125
- conv_gate: float32 [3, 5632], P(None, 'tp'), may hold values from -3.5 to 3.5
- conv_value: float32 [3, 5632], P(None, 'tp'), may hold values from -3.5 to 3.5
- w_down: bfloat16 [5632, 2048], P('tp', 'sp'), may hold values from -0.078125 to 0.078125
Outputs:
- layer_out: bfloat16 [32768, 2048], P(('sp', 'tp'))
All inputs are finite; a program needn't handle non-finite values.
Results may differ from a plain program's by a relative error of at most 0.012.
Values may be sent and summed in bfloat16 or wider, within the bound.
A program may use at most 128 MiB of HBM per device.

v0:
```python
import jax
import jax.numpy as jnp
from jax import lax
from jax.sharding import PartitionSpec as P

HEAD_DIM = 64
WINDOW = 128


def shifted(shard, axis, by):
    size = lax.axis_size(axis)
    pairs = [(i, i + by) for i in range(size) if 0 <= i + by < size]
    return lax.ppermute(shard, axis, pairs)


def joined_along(pieces, dim):
    shape = list(pieces.shape[1:])
    shape[dim] *= pieces.shape[0]
    return jnp.moveaxis(pieces, 0, dim).reshape(shape)


def sent_to_all(shard, axis):
    size = lax.axis_size(axis)
    return lax.all_to_all(
        jnp.broadcast_to(shard[None], (size, *shard.shape)), axis, 0, 0, tiled=True
    )


def gathered_copies(shard, axis, dim):
    return joined_along(sent_to_all(shard, axis), dim)


def side_by_side(arrays, axis, dim, along):
    both = jnp.concatenate(arrays, axis=along)
    out, at, done = (lax.all_gather(both, axis, axis=dim, tiled=True), 0, [])
    for a in arrays:
        done.append(lax.slice_in_dim(out, at, at + a.shape[along], axis=along))
        at += a.shape[along]
    return tuple(done)


def attend(query_rows, key_ext, value_ext, doc_rows, doc_ext, sinks):
    row_count = query_rows.shape[0]
    block_count = row_count // WINDOW
    kv_heads = key_ext.shape[1] // HEAD_DIM
    group_size = query_rows.shape[1] // (kv_heads * HEAD_DIM)

    def band(t):
        lower = t[:row_count].reshape((block_count, WINDOW) + t.shape[1:])
        upper = t[WINDOW:].reshape((block_count, WINDOW) + t.shape[1:])
        return jnp.concatenate([lower, upper], axis=1)

    query_band = query_rows.reshape(block_count, WINDOW, kv_heads, group_size, HEAD_DIM)
    key_band = band(key_ext).reshape(block_count, 2 * WINDOW, kv_heads, HEAD_DIM)
    value_band = band(value_ext).reshape(block_count, 2 * WINDOW, kv_heads, HEAD_DIM)
    doc_band = band(doc_ext)
    distance = jnp.arange(WINDOW)[:, None] + WINDOW - jnp.arange(2 * WINDOW)[None, :]
    in_window = (distance >= 0) & (distance < WINDOW)
    same_doc = doc_rows.reshape(block_count, WINDOW)[:, :, None] == doc_band[:, None, :]
    keep_mask = in_window[None] & same_doc
    scores = jnp.einsum(
        "nqhgd,nkhd->nhgqk", query_band, key_band, preferred_element_type=jnp.float32
    ) * HEAD_DIM ** (-0.5)
    scores = jnp.where(keep_mask[:, None, None], scores, -jnp.inf)
    sink_logit = sinks.reshape(kv_heads, group_size)[None, :, :, None, None]
    peak = jnp.maximum(jnp.max(scores, axis=-1, keepdims=True), sink_logit)
    expd = jnp.exp(scores - peak)
    probs = (expd / (jnp.sum(expd, axis=-1, keepdims=True) + jnp.exp(sink_logit - peak))).astype(
        jnp.bfloat16
    )
    mixed = jnp.einsum("nhgqk,nkhd->nqhgd", probs, value_band, preferred_element_type=jnp.float32)
    return mixed.astype(jnp.bfloat16).reshape(row_count, -1)


def convolve(ext_rows, doc_ext, taps):
    center = doc_ext[2:]
    same_one = (doc_ext[1:-1] == center)[:, None]
    same_two = (doc_ext[:-2] == center)[:, None]
    ext32 = ext_rows.astype(jnp.float32)
    result = taps[2] * ext32[2:]
    result = result + jnp.where(same_one, taps[1] * ext32[1:-1], 0.0)
    return result + jnp.where(same_two, taps[0] * ext32[:-2], 0.0)


def per_device(
    queries,
    keys,
    values,
    doc_ids,
    sinks,
    residual,
    out_weight,
    norm_gain,
    w_gate,
    w_value,
    conv_gate,
    conv_value,
    w_down,
):
    docs_plus = doc_ids + 1
    prev_keys, prev_values, prev_docs = shifted(
        (keys[-WINDOW:], values[-WINDOW:], docs_plus[-WINDOW:]), "sp", 1
    )
    key_ext = jnp.concatenate([prev_keys, keys], axis=0)
    value_ext = jnp.concatenate([prev_values, values], axis=0)
    doc_ext = jnp.concatenate([prev_docs, docs_plus], axis=0)
    head_out = attend(queries, key_ext, value_ext, docs_plus, doc_ext, sinks)
    head_rows = lax.all_to_all(head_out, "tp", split_axis=0, concat_axis=1, tiled=True)
    proj = jnp.dot(
        head_rows,
        lax.all_gather(out_weight, "tp", axis=0, tiled=True),
        preferred_element_type=jnp.float32,
    )
    mid32 = (residual.astype(jnp.float32) + proj).astype(jnp.bfloat16).astype(jnp.float32)
    normed = (
        mid32 * lax.rsqrt(jnp.mean(mid32 * mid32, axis=-1, keepdims=True) + 1e-06) * norm_gain
    ).astype(jnp.bfloat16)
    whole = gathered_copies(normed, "tp", 0)

    def add_rows(piece):
        return jnp.dot(whole, piece, preferred_element_type=jnp.float32)

    pieces = side_by_side((w_gate, w_value), "sp", 0, 1)
    gate_sum = add_rows(pieces[0])
    value_sum = add_rows(pieces[1])
    gate_pre = gate_sum.astype(jnp.bfloat16)
    value_pre = value_sum.astype(jnp.bfloat16)
    prev_gate, prev_value = shifted((gate_pre[-2:], value_pre[-2:]), "sp", 1)
    conv_docs = jnp.concatenate([prev_docs[-2:], docs_plus], axis=0)
    gate_conv = convolve(jnp.concatenate([prev_gate, gate_pre], axis=0), conv_docs, conv_gate)
    value_conv = convolve(jnp.concatenate([prev_value, value_pre], axis=0), conv_docs, conv_value)
    hidden = (jax.nn.silu(gate_conv) * value_conv).astype(jnp.bfloat16)
    terms = jnp.dot(
        hidden, lax.all_gather(w_down, "sp", axis=1, tiled=True), preferred_element_type=jnp.float32
    )
    sums = lax.psum_scatter(
        terms.astype(jnp.bfloat16), "tp", scatter_dimension=0, tiled=True
    ).astype(jnp.float32)
    return (mid32 + sums).astype(jnp.bfloat16)


def solution(mesh):
    return jax.shard_map(
        per_device,
        mesh=mesh,
        in_specs=(
            P("sp", "tp"),
            P("sp", "tp"),
            P("sp", "tp"),
            P("sp"),
            P("tp"),
            P(("sp", "tp"), None),
            P("tp", None),
            P(),
            P("sp", "tp"),
            P("sp", "tp"),
            P(None, "tp"),
            P(None, "tp"),
            P("tp", "sp"),
        ),
        out_specs=P(("sp", "tp"), None),
        check_vma=False,
    )
```

profile of v0, /device:TPU:1, one launch (start us, length us, event | category | flops | bytes accessed | tf_op | source)
XLA Modules:
  0.0 256.3 jit_solution(1870494783780439739)
XLA Ops:
  6.5 0.0 copy-start
  6.5 0.0 all-gather.4.cloned.1.call-start
  6.5 0.7 all-gather.4.cloned.1.call-update
  7.3 0.0 all-gather.6.cloned.1.call-start
  7.3 1.8 pad_maximum_fusion
  9.1 0.0 all-gather.6.cloned.1.call-update
  9.1 0.0 all-gather.8.cloned.1.call-start
  9.1 0.7 broadcast_add_fusion
  9.8 4.6 %collective-permute-start.1 = (s32[128]{0:T(128)S(1)}, s32[128]{0:T(128)S(1)}, u32[]{:S(2)}, u32[]{:S(2)}) collective-permute-start(s32[128]{0:T(128)S(1)} %slice.89), channel_id=1, source_target_pairs={{0,4},{4,8},{8,12},{12,16},{16,20},{20,24},{24,28},{28,32},{32,36}... | collective-permute-start | bytes 1544 | tf_op jit(solution)/shard_map/ppermute | solution.py:13
  14.4 0.7 slice.92
  15.2 1.9 collective-permute-start.2
  17.1 0.7 slice.87
  17.8 3.6 %collective-permute-start = (bf16[128,64]{0,1:T(8,128)(2,1)S(1)}, bf16[128,64]{0,1:T(8,128)(2,1)S(1)}, u32[]{:S(2)}, u32[]{:S(2)}) collective-permute-start(bf16[128,64]{0,1:T(8,128)(2,1)S(1)} %slice.87), channel_id=1, source_target_pairs={{0,4},{4,8},{8,12},{12,16},{16,20},{20,24},{24,28},{28,32},{32,36}... | collective-permute-start | bytes 49160 | tf_op jit(solution)/shard_map/ppermute | solution.py:13
  21.4 0.0 all-gather.8.cloned.1.call-update
  21.4 1.0 copy_bitcast_fusion
  22.4 0.0 copy-start.5
  22.4 1.0 copy_bitcast_fusion.2
  23.4 2.1 reshape.131
  25.5 0.0 collective-permute-done.1
  25.5 0.3 compare_and_fusion
  25.9 0.0 collective-permute-done.2
  25.9 0.0 copy-done
  25.9 0.0 copy-start.1
  25.9 0.9 fusion.21
  26.8 0.0 copy-done.5
  26.8 0.1 broadcast_maximum_fusion
  26.9 1.0 fusion.20
  27.9 0.1 exponential_add_fusion
  28.0 0.0 collective-permute-done
  28.0 0.0 copy-done.1
  28.0 1.2 fusion.34
  29.2 0.3 copy.32
  29.6 0.3 all_to_all.17
  29.9 0.1 copy.33
  30.0 19.1 %all_to_all.24 = bf16[4,256,256]{1,2,0:T(8,128)(2,1)S(1)} all-to-all(bf16[4,256,256]{1,2,0:T(8,128)(2,1)S(1)} %copy.33), channel_id=1, replica_groups=mesh['sp'=32,'tp'=4] {'tp'}, dimensions={0} | all-to-all | bytes 1048576 | tf_op jit(solution)/shard_map/all_to_all | solution.py:108
  49.1 16.7 %all-gather.4.cloned.1.call-done = bf16[1024,2048]{1,0:T(8,128)(2,1)} async-done(((bf16[256,2048]{1,0:T(8,128)(2,1)}), bf16[1024,2048]{1,0:T(8,128)(2,1)}) %all-gather.4.cloned.1.call-update) | async-done | bytes 4194320 | tf_op jit(solution)/shard_map/all_gather | solution.py:111
  65.8 0.0 copy-done.7
  65.8 3.6 %fusion.24 = (f32[256]{0:T(256)S(1)}, bf16[256,2048]{1,0:T(8,128)(2,1)S(1)}) fusion(bf16[256,1024]{0,1:T(8,128)(2,1)S(1)} %bitcast.77, bf16[1024,2048]{1,0:T(8,128)(2,1)} %all-gather.4.cloned.1.call-done, bf16[256,2048]{1,0:T(8,128)(2,1)S(1)} %copy-done.7), kind=kOutput, calls=%fused_computation.35 | convolution fusion | flops 1076887296 | bytes 6816768 | tf_op jit(solution)/shard_map/dot_general | solution.py:109
  69.5 0.0 copy-done.4
  69.5 0.3 fusion.26
  69.8 2.6 broadcast_in_dim.59
  72.3 5.0 %all-to-all-start.1 = ((bf16[4,256,2048]{2,1,0:T(8,128)(2,1)}), bf16[4,256,2048]{2,1,0:T(8,128)(2,1)}, u32[]{:S(2)}, u32[]{:S(2)}) async-start(bf16[4,256,2048]{2,1,0:T(8,128)(2,1)} %broadcast_in_dim.59), calls=%async_computation.1 | async-start | bytes 8388608 | tf_op jit(solution)/shard_map/all_to_all | solution.py:24
  77.3 0.0 reduce-scatter.2.cloned.1.call-start
  77.4 0.0 copy-done.2
  77.4 0.0 copy-done.3
  77.4 0.1 slice_reduce_fusion.2
  77.5 0.1 slice.98
  77.6 0.1 fusion.49
  77.7 47.8 %all-to-all-done.1 = bf16[4,256,2048]{2,1,0:T(8,128)(2,1)} async-done(((bf16[4,256,2048]{2,1,0:T(8,128)(2,1)}), bf16[4,256,2048]{2,1,0:T(8,128)(2,1)}, u32[]{:S(2)}, u32[]{:S(2)}) %all-to-all-start.1) | async-done | bytes 4194336 | tf_op jit(solution)/shard_map/all_to_all | solution.py:24
  125.5 3.9 %all-gather.6.cloned.1.call-done = bf16[2048,2816]{1,0:T(8,128)(2,1)} async-done(((bf16[64,2816]{1,0:T(8,128)(2,1)}), bf16[2048,2816]{1,0:T(8,128)(2,1)}) %all-gather.6.cloned.1.call-update) | async-done | bytes 11534352 | tf_op jit(solution)/shard_map/all_gather | solution.py:35
  129.3 10.3 %fusion.14 = bf16[1024,1408]{1,0:T(8,128)(2,1)S(1)} fusion(bf16[1024,2048]{1,0:T(8,128)(2,1)} %bitcast.13, bf16[2048,2816]{1,0:T(8,128)(2,1)} %all-gather.6.cloned.1.call-done), kind=kOutput, calls=%fused_computation.23 | convolution fusion | flops 5907021824 | bytes 12845056 | tf_op jit(solution)/shard_map/dot_general | solution.py:121
  139.6 3.4 %collective-permute-start.3 = (bf16[2,1408]{1,0:T(2,128)(2,1)S(1)}, bf16[2,1408]{1,0:T(2,128)(2,1)S(1)}, u32[]{:S(2)}, u32[]{:S(2)}) collective-permute-start(bf16[2,1408]{1,0:T(2,128)(2,1)S(1)} %slice.114), channel_id=1, source_target_pairs={{0,4},{4,8},{8,12},{12,16},{16,20},{20,24},{24,28},{28,32},{32,36}... | collective-permute-start | bytes 16904 | tf_op jit(solution)/shard_map/ppermute | solution.py:13
  143.1 0.0 copy-done.6
  143.1 8.5 %fusion.17 = bf16[1024,1408]{1,0:T(8,128)(2,1)S(1)} fusion(bf16[1024,2048]{1,0:T(8,128)(2,1)} %bitcast.13, bf16[2048,2816]{1,0:T(8,128)(2,1)S(1)} %copy-done.6), kind=kOutput, calls=%fused_computation.24 | convolution fusion | flops 5907021824 | bytes 12845056 | tf_op jit(solution)/shard_map/dot_general | solution.py:121
  151.6 2.2 collective-permute-start.4
  153.8 0.0 collective-permute-done.3
  153.8 3.0 %maximum_convert_fusion = f32[1026,1408]{1,0:T(8,128)} fusion(bf16[1024,1408]{1,0:T(8,128)(2,1)S(1)} %fusion.14, bf16[2,1408]{1,0:T(2,128)(2,1)S(1)} %collective-permute-done.3), kind=kLoop, calls=%fused_computation.31 | loop fusion | flops 5778432 | bytes 8667648 | tf_op jit(solution)/shard_map/convert_element_type | solution.py:79
  156.8 0.0 collective-permute-done.4
  156.8 3.1 %maximum_convert_fusion.1 = f32[1026,1408]{1,0:T(8,128)} fusion(bf16[1024,1408]{1,0:T(8,128)(2,1)S(1)} %fusion.17, bf16[2,1408]{1,0:T(2,128)(2,1)S(1)} %collective-permute-done.4), kind=kLoop, calls=%fused_computation.32 | loop fusion | flops 5778432 | bytes 8667648 | tf_op jit(solution)/shard_map/convert_element_type | solution.py:79
  159.9 19.4 %all-gather.8.cloned.1.call-done = bf16[1408,2048]{0,1:T(8,128)(2,1)} async-done(((bf16[1408,64]{0,1:T(8,128)(2,1)}), bf16[1408,2048]{0,1:T(8,128)(2,1)}) %all-gather.8.cloned.1.call-update) | async-done | bytes 5767184 | tf_op jit(solution)/shard_map/all_gather | solution.py:134
  179.3 22.3 %convolution_convert_fusion = bf16[1024,2048]{1,0:T(8,128)(2,1)} fusion(bf16[1408,2048]{0,1:T(8,128)(2,1)} %all-gather.8.cloned.1.call-done, f32[1026,1408]{1,0:T(8,128)} %maximum_convert_fusion.1, f32[1026,1408]{1,0:T(8,128)} %maximum_convert_fusion, f32[1408]{0:T(1024)S(1)} %get-tuple-element.9, f32[1408]{0:T(1024)S(1)} %get-tuple-element.10, ...), kind=kOutput, calls=%fused_computation.25 | convolution fusion | flops 5936513024 | bytes 44600320 | tf_op jit(solution)/shard_map/dot_general | solution.py:133
  201.7 0.0 reduce-scatter.2.cloned.1.call-update
  201.7 45.4 %reduce-scatter.2.cloned.1.call-done = bf16[256,2048]{1,0:T(8,128)(2,1)} async-done(((bf16[1024,2048]{1,0:T(8,128)(2,1)}), bf16[256,2048]{1,0:T(8,128)(2,1)}) %reduce-scatter.2.cloned.1.call-update) | async-done | bytes 1048592 | tf_op jit(solution)/shard_map/reduce_scatter | solution.py:136
  247.1 2.6 %fusion.27 = bf16[256,2048]{1,0:T(8,128)(2,1)} fusion(bf16[256,2048]{1,0:T(8,128)(2,1)S(1)} %get-tuple-element.18, bf16[256,2048]{1,0:T(8,128)(2,1)} %reduce-scatter.2.cloned.1.call-done), kind=kLoop, calls=%fused_computation.38 | loop fusion | flops 2097152 | bytes 3145728 | tf_op jit(solution)/shard_map/convert_element_type | solution.py:139
  (15 shorter events, 0.1 us)
Async XLA Ops:
  6.5 19.3 %copy-start = (bf16[1024,64]{0,1:T(8,128)(2,1)S(1)}, bf16[1024,64]{0,1:T(8,128)(2,1)}, u32[]{:S(2)}) copy-start(bf16[1024,64]{0,1:T(8,128)(2,1)} %param.14) | copy-start | bytes 393220
  6.5 59.3 %all-gather.4.cloned.1.call-start = ((), (), s32[]{:S(2)}) async-start(), calls=%async_computation.3 | async-start | bytes 5242880 | tf_op jit(solution)/shard_map/all_gather | solution.py:111
  7.3 122.1 %all-gather.6.cloned.1.call-start = ((), (), s32[]{:S(2)}) async-start(), calls=%async_computation.4 | async-start | bytes 11894784 | tf_op jit(solution)/shard_map/all_gather | solution.py:35
  9.1 170.2 %all-gather.8.cloned.1.call-start = ((), (), s32[]{:S(2)}) async-start(), calls=%async_computation.5 | async-start | bytes 5947392 | tf_op jit(solution)/shard_map/all_gather | solution.py:134
  9.8 15.6 %collective-permute-start.1 = (s32[128]{0:T(128)S(1)}, s32[128]{0:T(128)S(1)}, u32[]{:S(2)}, u32[]{:S(2)}) collective-permute-start(s32[128]{0:T(128)S(1)} %slice.89), channel_id=1, source_target_pairs={{0,4},{4,8},{8,12},{12,16},{16,20},{20,24},{24,28},{28,32},{32,36}... | collective-permute-start | bytes 1544 | tf_op jit(solution)/shard_map/ppermute | solution.py:13
  15.2 10.7 %collective-permute-start.2 = (bf16[128,64]{0,1:T(8,128)(2,1)S(1)}, bf16[128,64]{0,1:T(8,128)(2,1)S(1)}, u32[]{:S(2)}, u32[]{:S(2)}) collective-permute-start(bf16[128,64]{0,1:T(8,128)(2,1)S(1)} %slice.92), channel_id=1, source_target_pairs={{0,4},{4,8},{8,12},{12,16},{16,20},{20,24},{24,28},{28,32},{32,36}... | collective-permute-start | bytes 49160 | tf_op jit(solution)/shard_map/ppermute | solution.py:13
  17.8 10.2 %collective-permute-start = (bf16[128,64]{0,1:T(8,128)(2,1)S(1)}, bf16[128,64]{0,1:T(8,128)(2,1)S(1)}, u32[]{:S(2)}, u32[]{:S(2)}) collective-permute-start(bf16[128,64]{0,1:T(8,128)(2,1)S(1)} %slice.87), channel_id=1, source_target_pairs={{0,4},{4,8},{8,12},{12,16},{16,20},{20,24},{24,28},{28,32},{32,36}... | collective-permute-start | bytes 49160 | tf_op jit(solution)/shard_map/ppermute | solution.py:13
  22.4 4.5 %copy-start.5 = (f32[4]{0:T(128)S(1)}, f32[4]{0:T(128)}, u32[]{:S(2)}) copy-start(f32[4]{0:T(128)} %param.17) | copy-start | bytes 52
  25.9 2.1 copy-start.1
  29.2 36.6 %copy-start.7 = (bf16[256,2048]{1,0:T(8,128)(2,1)S(1)}, bf16[256,2048]{1,0:T(8,128)(2,1)}, u32[]{:S(2)}) copy-start(bf16[256,2048]{1,0:T(8,128)(2,1)} %param.18) | copy-start | bytes 3145732
  49.1 20.3 %copy-start.4 = (f32[2048]{0:T(1024)S(1)}, f32[2048]{0:T(1024)}, u32[]{:S(2)}) copy-start(f32[2048]{0:T(1024)} %param.20) | copy-start | bytes 24580
  72.3 5.0 %copy-start.2 = (f32[3,1408]{1,0:T(4,128)S(1)}, f32[3,1408]{1,0:T(4,128)}, u32[]{:S(2)}) copy-start(f32[3,1408]{1,0:T(4,128)} %param.24) | copy-start | bytes 50692
  72.3 5.1 %copy-start.3 = (f32[3,1408]{1,0:T(4,128)S(1)}, f32[3,1408]{1,0:T(4,128)}, u32[]{:S(2)}) copy-start(f32[3,1408]{1,0:T(4,128)} %param.23) | copy-start | bytes 50692
  72.3 53.1 %all-to-all-start.1 = ((bf16[4,256,2048]{2,1,0:T(8,128)(2,1)}), bf16[4,256,2048]{2,1,0:T(8,128)(2,1)}, u32[]{:S(2)}, u32[]{:S(2)}) async-start(bf16[4,256,2048]{2,1,0:T(8,128)(2,1)} %broadcast_in_dim.59), calls=%async_computation.1 | async-start | bytes 8388608 | tf_op jit(solution)/shard_map/all_to_all | solution.py:24
  77.3 169.8 %reduce-scatter.2.cloned.1.call-start = ((), (), s32[]{:S(2)}) async-start(), calls=%async_computation.6 | async-start | bytes 5242880 | tf_op jit(solution)/shard_map/reduce_scatter | solution.py:136
  129.3 13.7 %copy-start.6 = (bf16[2048,2816]{1,0:T(8,128)(2,1)S(1)}, bf16[2048,2816]{1,0:T(8,128)(2,1)}, u32[]{:S(2)}) copy-start(bf16[2048,2816]{1,0:T(8,128)(2,1)} %all-gather.6.cloned.1.call-done) | copy-start | bytes 34603012
  139.6 14.1 %collective-permute-start.3 = (bf16[2,1408]{1,0:T(2,128)(2,1)S(1)}, bf16[2,1408]{1,0:T(2,128)(2,1)S(1)}, u32[]{:S(2)}, u32[]{:S(2)}) collective-permute-start(bf16[2,1408]{1,0:T(2,128)(2,1)S(1)} %slice.114), channel_id=1, source_target_pairs={{0,4},{4,8},{8,12},{12,16},{16,20},{20,24},{24,28},{28,32},{32,36}... | collective-permute-start | bytes 16904 | tf_op jit(solution)/shard_map/ppermute | solution.py:13
  151.6 5.2 %collective-permute-start.4 = (bf16[2,1408]{1,0:T(2,128)(2,1)S(1)}, bf16[2,1408]{1,0:T(2,128)(2,1)S(1)}, u32[]{:S(2)}, u32[]{:S(2)}) collective-permute-start(bf16[2,1408]{1,0:T(2,128)(2,1)S(1)} %slice.121), channel_id=1, source_target_pairs={{0,4},{4,8},{8,12},{12,16},{16,20},{20,24},{24,28},{28,32},{32,36}... | collective-permute-start | bytes 16904 | tf_op jit(solution)/shard_map/ppermute | solution.py:13
Sparse Core Ops, SparseCore 0:
  9.0 56.8 all-gather.3
  68.1 61.1 all-gather.5
  131.6 47.7 all-gather.7
  201.8 45.2 reduce-scatter.1
where the time goes:
time: 257 us; the launch traced here: 256 us
  waiting for transfers between devices  134 us (52%)
  matrix products  46.8 us (18%)
  starting transfers between devices  20.8 us (8%)
  blocking collectives  19.1 us (7%)
  between operations  13.4 us (5%)
  other arithmetic  13.2 us (5%)
  local copies, waits for them, and re-layouts  8.96 us (3%)
    all_to_all x1, waiting for transfers between devices, sent_to_all(): lax.all_to_all(jnp.broadcast_to(shard[None], (size, *shard.shape)), axis,...  47.8 us
    reduce_scatter x1, waiting for transfers between devices, per_device(): lax.psum_scatter(terms.astype(jnp.bfloat16), 'tp', scatter_dimension=0, t...  45.4 us
    dot_general x1, matrix products, per_device(): jnp.dot(hidden, lax.all_gather(w_down, 'sp', axis=1, tiled=True), preferr...  22.3 us
    all_gather x1, waiting for transfers between devices, per_device(): lax.all_gather(w_down, 'sp', axis=1, tiled=True)  19.4 us
    all_to_all x1, blocking collectives, per_device(): lax.all_to_all(head_out, 'tp', split_axis=0, concat_axis=1, tiled=True)  19.1 us
    dot_general x2, matrix products, add_rows(): return jnp.dot(whole, piece, preferred_element_type=jnp.float32)  18.7 us
    all_gather x1, waiting for transfers between devices, per_device(): lax.all_gather(out_weight, 'tp', axis=0, tiled=True)  16.7 us
    ppermute x5, starting transfers between devices, shifted(): return lax.ppermute(shard, axis, pairs)  15.7 us
  transfers between devices with their start and end apart: 10, of which 5 were waited for; matrix products, arithmetic and copies ran while one was open for 17% of the time, Pallas kernels for 0%

commit v1 on v0

--- a/solution.py
+++ b/solution.py
@@ -1,3 +1,4 @@
+import functools
 import jax
 import jax.numpy as jnp
 from jax import lax
@@ -5,6 +6,36 @@
 
 HEAD_DIM = 64
 WINDOW = 128
+
+
+def wait_leaf_for(matrix, d_out):
+    latest, far_arr, row_out = (
+        jax.lax.axis_size("tp"),
+        jax.lax.axis_index("tp"),
+        matrix.shape[d_out],
+    )
+    in_order = [(h, (h + 1) % latest) for h in range(latest)]
+    sheets = [(h, (h - 1) % latest) for h in range(latest)]
+    val = jnp.zeros(
+        (*matrix.shape[:d_out], latest * row_out, *matrix.shape[d_out + 1 :]), matrix.dtype
+    )
+    val = lax.dynamic_update_slice_in_dim(val, matrix, far_arr * row_out, axis=d_out)
+    odd = arr_now = matrix
+    w2 = latest // 2
+    for j in tuple(range(1, w2 + 1)):
+        odd = jax.lax.ppermute(odd, "tp", in_order)
+        val = lax.dynamic_update_slice_in_dim(
+            val, odd, (far_arr - j) % latest * row_out, axis=d_out
+        )
+        if j < latest - w2:
+            arr_now = jax.lax.ppermute(arr_now, "tp", sheets)
+            val = lax.dynamic_update_slice_in_dim(
+                val, arr_now, (far_arr + j) % latest * row_out, axis=d_out
+            )
+    return val
+
+
+slots_build = functools.partial(wait_leaf_for, d_out=0)
 
 
 def shifted(shard, axis, by):
@@ -106,11 +137,7 @@
     doc_ext = jnp.concatenate([prev_docs, docs_plus], axis=0)
     head_out = attend(queries, key_ext, value_ext, docs_plus, doc_ext, sinks)
     head_rows = lax.all_to_all(head_out, "tp", split_axis=0, concat_axis=1, tiled=True)
-    proj = jnp.dot(
-        head_rows,
-        lax.all_gather(out_weight, "tp", axis=0, tiled=True),
-        preferred_element_type=jnp.float32,
-    )
+    proj = jnp.dot(head_rows, slots_build(out_weight), preferred_element_type=jnp.float32)
     mid32 = (residual.astype(jnp.float32) + proj).astype(jnp.bfloat16).astype(jnp.float32)
     normed = (
         mid32 * lax.rsqrt(jnp.mean(mid32 * mid32, axis=-1, keepdims=True) + 1e-06) * norm_gain

time: 257 us -> 238 us (0.926)
  waiting for transfers between devices: 134 us -> 114 us
  blocking collectives: 19.1 us -> 0 us
  local copies, waits for them, and re-layouts: 8.96 us -> 19.1 us
  starting transfers between devices: 20.8 us -> 29.6 us
    all_gather x1, waiting for transfers between devices: 19.4 us -> 0.01 us  [per_device(): lax.all_gather(w_down, 'sp', axis=1, tiled=True)]
    all_to_all x1 -> x0, blocking collectives: 19.1 us -> none  [per_device(): lax.all_to_all(head_out, 'tp', split_axis=0, concat_axis=1, tiled=True)]
    all_gather x1 -> x0, waiting for transfers between devices: 16.7 us -> none  [per_device(): lax.all_gather(out_weight, 'tp', axis=0, tiled=True)]
    ppermute x0 -> x3, waiting for transfers between devices: none -> 15.8 us  [the longest x2 15.8 us: wait_leaf_for(): odd = jax.lax.ppermute(odd, 'tp', in_order)]
    dynamic_update_slice x0 -> x4, local copies, waits for them, and re-layouts: none -> 5.47 us  [the longest x1 2.32 us: wait_leaf_for(): lax.dynamic_update_slice_in_dim(val, arr_now, (far_arr + j) % latest * ro...]
    all_to_all x0 -> x1, waiting for transfers between devices: none -> 4.01 us  [per_device(): lax.all_to_all(head_out, 'tp', split_axis=0, concat_axis=1, tiled=True)]
    all_to_all x0 -> x1, starting transfers between devices: none -> 3.93 us  [per_device(): lax.all_to_all(head_out, 'tp', split_axis=0, concat_axis=1, tiled=True)]
    all_gather x1, waiting for transfers between devices: 3.88 us -> 0.01 us  [side_by_side(): out, at, done = (lax.all_gather(both, axis, axis=dim, tiled=True), 0, [])]
  transfers between devices with their start and end apart: 10 -> 13, of which waited for: 5 -> 4; matrix products, arithmetic and copies ran while one was open for 17% -> 22% of each run, Pallas kernels for 0% -> 0%
where the time goes in v1:
time: 238 us; the launch traced here: 237 us
  waiting for transfers between devices  114 us (48%)
  matrix products  48.1 us (20%)
  starting transfers between devices  29.6 us (12%)
  local copies, waits for them, and re-layouts  19.1 us (8%)
  between operations  13.5 us (6%)
  other arithmetic  13.3 us (6%)
    reduce_scatter x1, waiting for transfers between devices, per_device(): lax.psum_scatter(terms.astype(jnp.bfloat16), 'tp', scatter_dimension=0, t...  47.2 us
    all_to_all x1, waiting for transfers between devices, sent_to_all(): lax.all_to_all(jnp.broadcast_to(shard[None], (size, *shard.shape)), axis,...  46.9 us
    dot_general x1, matrix products, per_device(): jnp.dot(hidden, lax.all_gather(w_down, 'sp', axis=1, tiled=True), preferr...  22.2 us
    dot_general x2, matrix products, add_rows(): return jnp.dot(whole, piece, preferred_element_type=jnp.float32)  18.7 us
    ppermute x5, starting transfers between devices, shifted(): return lax.ppermute(shard, axis, pairs)  16.9 us
    ppermute x2, waiting for transfers between devices, wait_leaf_for(): odd = jax.lax.ppermute(odd, 'tp', in_order)  15.8 us
    convert_element_type x2, other arithmetic, convolve(): ext32 = ext_rows.astype(jnp.float32)  6.13 us
    all_to_all x1, starting transfers between devices, sent_to_all(): lax.all_to_all(jnp.broadcast_to(shard[None], (size, *shard.shape)), axis,...  5.02 us
  transfers between devices with their start and end apart: 13, of which 4 were waited for; matrix products, arithmetic and copies ran while one was open for 22% of the time, Pallas kernels for 0%

profile of v1, /device:TPU:1, one launch (start us, length us, event | category | flops | bytes accessed | tf_op | source)
XLA Modules:
  0.0 237.4 jit_solution(12315375384478062412)
XLA Ops:
  6.5 1.9 pad_maximum_fusion
  8.4 0.0 all-gather.3.cloned.1.call-update
  8.4 0.0 all-gather.5.cloned.1.call-start
  8.5 2.1 collective-permute-start.3
  10.6 1.4 collective-permute-start.4
  11.9 0.7 broadcast_add_fusion
  12.6 4.4 %collective-permute-start.1 = (s32[128]{0:T(128)S(1)}, s32[128]{0:T(128)S(1)}, u32[]{:S(2)}, u32[]{:S(2)}) collective-permute-start(s32[128]{0:T(128)S(1)} %slice.89), channel_id=1, source_target_pairs={{0,4},{4,8},{8,12},{12,16},{16,20},{20,24},{24,28},{28,32},{32,36}... | collective-permute-start | bytes 1544 | tf_op jit(solution)/shard_map/ppermute | solution.py:44
  17.1 0.7 slice.92
  17.8 1.9 collective-permute-start.2
  19.7 0.7 slice.87
  20.4 3.6 %collective-permute-start = (bf16[128,64]{0,1:T(8,128)(2,1)S(1)}, bf16[128,64]{0,1:T(8,128)(2,1)S(1)}, u32[]{:S(2)}, u32[]{:S(2)}) collective-permute-start(bf16[128,64]{0,1:T(8,128)(2,1)S(1)} %slice.87), channel_id=1, source_target_pairs={{0,4},{4,8},{8,12},{12,16},{16,20},{20,24},{24,28},{28,32},{32,36}... | collective-permute-start | bytes 49160 | tf_op jit(solution)/shard_map/ppermute | solution.py:44
  24.0 0.0 all-gather.5.cloned.1.call-update
  24.1 1.6 copy_bitcast_fusion
  25.7 1.0 copy_bitcast_fusion.2
  26.7 2.5 %broadcast_in_dim.62 = bf16[1024,2048]{1,0:T(8,128)(2,1)} broadcast(bf16[]{:T(256)} %constant.47.clone.1), dimensions={} | broadcast | bytes 4194306 | tf_op jit(solution)/shard_map/broadcast_in_dim | solution.py:19
  29.2 1.1 constant_dynamic-update-slice_fusion.3
  30.3 2.0 reshape.131
  32.4 0.0 collective-permute-done.1
  32.4 0.3 compare_and_fusion
  32.7 0.0 collective-permute-done.2
  32.8 0.0 copy-start.2
  32.8 1.9 fusion.21
  34.7 0.1 broadcast_maximum_fusion
  34.7 1.0 fusion.20
  35.8 0.1 exponential_add_fusion
  35.8 0.0 collective-permute-done
  35.9 0.0 collective-permute-done.3
  35.9 0.1 collective-permute-start.5
  36.0 1.2 fusion.34
  37.2 0.3 copy.32
  37.6 0.3 all_to_all.17
  37.9 0.9 copy.33
  38.8 3.9 %all-to-all-start = ((bf16[4,256,256]{1,2,0:T(8,128)(2,1)}), bf16[4,256,256]{1,2,0:T(8,128)(2,1)S(1)}, u32[]{:S(2)}, u32[]{:S(2)}) async-start(bf16[4,256,256]{1,2,0:T(8,128)(2,1)} %copy.33), calls=%async_computation | async-start | bytes 1048576 | tf_op jit(solution)/shard_map/all_to_all | solution.py:139
  42.7 1.0 constant_dynamic-update-slice_fusion.2
  43.7 0.0 collective-permute-done.4
  43.7 2.3 constant_dynamic-update-slice_fusion.1
  46.0 15.8 %collective-permute-done.5 = bf16[256,2048]{1,0:T(8,128)(2,1)S(1)} collective-permute-done((bf16[256,2048]{1,0:T(8,128)(2,1)S(1)}, bf16[256,2048]{1,0:T(8,128)(2,1)S(1)}, u32[]{:S(2)}, u32[]{:S(2)}) %collective-permute-start.5) | collective-permute-done | bytes 1048608 | tf_op jit(solution)/shard_map/ppermute | solution.py:26
  61.8 1.0 constant_dynamic-update-slice_fusion
  62.9 4.0 %all-to-all-done = bf16[4,256,256]{1,2,0:T(8,128)(2,1)S(1)} async-done(((bf16[4,256,256]{1,2,0:T(8,128)(2,1)}), bf16[4,256,256]{1,2,0:T(8,128)(2,1)S(1)}, u32[]{:S(2)}, u32[]{:S(2)}) %all-to-all-start) | async-done | bytes 524320 | tf_op jit(solution)/shard_map/all_to_all | solution.py:139
  66.9 0.8 copy-done.3
  67.7 4.1 %fusion.24 = (f32[256]{0:T(256)S(1)}, bf16[256,2048]{1,0:T(8,128)(2,1)S(1)}) fusion(bf16[256,1024]{0,1:T(8,128)(2,1)} %bitcast.77, bf16[1024,2048]{1,0:T(8,128)(2,1)} %constant_dynamic-update-slice_fusion, bf16[256,2048]{1,0:T(8,128)(2,1)} %param.18), kind=kOutput, calls=%fused_computation.35 | convolution fusion | flops 1076887296 | bytes 6816768 | tf_op jit(solution)/shard_map/dot_general | solution.py:140
  71.8 0.3 fusion.26
  72.1 2.5 %broadcast_in_dim.63 = bf16[4,256,2048]{2,1,0:T(8,128)(2,1)} broadcast(bf16[256,2048]{1,0:T(8,128)(2,1)S(1)} %fusion.26), dimensions={1,2} | broadcast | bytes 5242880 | tf_op jit(solution)/shard_map/broadcast_in_dim | solution.py:56
  74.6 5.0 %all-to-all-start.1 = ((bf16[4,256,2048]{2,1,0:T(8,128)(2,1)}), bf16[4,256,2048]{2,1,0:T(8,128)(2,1)}, u32[]{:S(2)}, u32[]{:S(2)}) async-start(bf16[4,256,2048]{2,1,0:T(8,128)(2,1)} %broadcast_in_dim.63), calls=%async_computation.1 | async-start | bytes 8388608 | tf_op jit(solution)/shard_map/all_to_all | solution.py:55
  79.7 0.2 reduce-scatter.2.cloned.1.call-start
  79.9 0.0 copy-done.4
  79.9 0.0 copy-done.5
  79.9 0.1 slice_reduce_fusion.2
  80.0 0.1 slice.98
  80.1 0.1 fusion.49
  80.2 46.9 %all-to-all-done.1 = bf16[4,256,2048]{2,1,0:T(8,128)(2,1)} async-done(((bf16[4,256,2048]{2,1,0:T(8,128)(2,1)}), bf16[4,256,2048]{2,1,0:T(8,128)(2,1)}, u32[]{:S(2)}, u32[]{:S(2)}) %all-to-all-start.1) | async-done | bytes 4194336 | tf_op jit(solution)/shard_map/all_to_all | solution.py:55
  127.0 10.3 %fusion.14 = bf16[1024,1408]{1,0:T(8,128)(2,1)S(1)} fusion(bf16[1024,2048]{1,0:T(8,128)(2,1)} %bitcast.13, bf16[2048,2816]{1,0:T(8,128)(2,1)} %all-gather.3.cloned.1.call-done), kind=kOutput, calls=%fused_computation.23 | convolution fusion | flops 5907021824 | bytes 12845056 | tf_op jit(solution)/shard_map/dot_general | solution.py:148
  137.3 5.0 %collective-permute-start.6 = (bf16[2,1408]{1,0:T(2,128)(2,1)S(1)}, bf16[2,1408]{1,0:T(2,128)(2,1)S(1)}, u32[]{:S(2)}, u32[]{:S(2)}) collective-permute-start(bf16[2,1408]{1,0:T(2,128)(2,1)S(1)} %slice.114), channel_id=1, source_target_pairs={{0,4},{4,8},{8,12},{12,16},{16,20},{20,24},{24,28},{28,32},{32,36}... | collective-permute-start | bytes 16904 | tf_op jit(solution)/shard_map/ppermute | solution.py:44
  142.3 0.0 copy-done.8
  142.4 8.5 %fusion.17 = bf16[1024,1408]{1,0:T(8,128)(2,1)S(1)} fusion(bf16[1024,2048]{1,0:T(8,128)(2,1)} %bitcast.13, bf16[2048,2816]{1,0:T(8,128)(2,1)S(1)} %copy-done.8), kind=kOutput, calls=%fused_computation.24 | convolution fusion | flops 5907021824 | bytes 12845056 | tf_op jit(solution)/shard_map/dot_general | solution.py:148
  150.9 1.9 collective-permute-start.7
  152.8 0.0 collective-permute-done.6
  152.8 3.0 %maximum_convert_fusion = f32[1026,1408]{1,0:T(8,128)} fusion(bf16[1024,1408]{1,0:T(8,128)(2,1)S(1)} %fusion.14, bf16[2,1408]{1,0:T(2,128)(2,1)S(1)} %collective-permute-done.6), kind=kLoop, calls=%fused_computation.31 | loop fusion | flops 5778432 | bytes 8667648 | tf_op jit(solution)/shard_map/convert_element_type | solution.py:110
  155.8 0.0 collective-permute-done.7
  155.8 3.1 %maximum_convert_fusion.1 = f32[1026,1408]{1,0:T(8,128)} fusion(bf16[1024,1408]{1,0:T(8,128)(2,1)S(1)} %fusion.17, bf16[2,1408]{1,0:T(2,128)(2,1)S(1)} %collective-permute-done.7), kind=kLoop, calls=%fused_computation.32 | loop fusion | flops 5778432 | bytes 8667648 | tf_op jit(solution)/shard_map/convert_element_type | solution.py:110
  158.9 22.2 %convolution_convert_fusion = bf16[1024,2048]{1,0:T(8,128)(2,1)} fusion(bf16[1408,2048]{0,1:T(8,128)(2,1)} %all-gather.5.cloned.1.call-done, f32[1026,1408]{1,0:T(8,128)} %maximum_convert_fusion.1, f32[1026,1408]{1,0:T(8,128)} %maximum_convert_fusion, f32[1408]{0:T(1024)S(1)} %get-tuple-element.9, f32[1408]{0:T(1024)S(1)} %get-tuple-element.10, ...), kind=kOutput, calls=%fused_computation.25 | convolution fusion | flops 5936513024 | bytes 44600320 | tf_op jit(solution)/shard_map/dot_general | solution.py:160
  181.1 0.0 reduce-scatter.2.cloned.1.call-update
  181.1 47.2 %reduce-scatter.2.cloned.1.call-done = bf16[256,2048]{1,0:T(8,128)(2,1)} async-done(((bf16[1024,2048]{1,0:T(8,128)(2,1)}), bf16[256,2048]{1,0:T(8,128)(2,1)}) %reduce-scatter.2.cloned.1.call-update) | async-done | bytes 1048592 | tf_op jit(solution)/shard_map/reduce_scatter | solution.py:163
  228.3 2.6 %fusion.27 = bf16[256,2048]{1,0:T(8,128)(2,1)} fusion(bf16[256,2048]{1,0:T(8,128)(2,1)S(1)} %get-tuple-element.18, bf16[256,2048]{1,0:T(8,128)(2,1)} %reduce-scatter.2.cloned.1.call-done), kind=kLoop, calls=%fused_computation.38 | loop fusion | flops 2097152 | bytes 3145728 | tf_op jit(solution)/shard_map/convert_element_type | solution.py:166
  (26 shorter events, 0.2 us)
Async XLA Ops:
  6.5 22.7 %copy-start = (bf16[256,2048]{1,0:T(8,128)(2,1)S(1)}, bf16[256,2048]{1,0:T(8,128)(2,1)}, u32[]{:S(2)}) copy-start(bf16[256,2048]{1,0:T(8,128)(2,1)} %param.19) | copy-start | bytes 3145732
  6.5 120.5 %all-gather.3.cloned.1.call-start = ((), (), s32[]{:S(2)}) async-start(), calls=%async_computation.3 | async-start | bytes 11894784 | tf_op jit(solution)/shard_map/all_gather | solution.py:66
  8.4 150.5 %all-gather.5.cloned.1.call-start = ((), (), s32[]{:S(2)}) async-start(), calls=%async_computation.4 | async-start | bytes 5947392 | tf_op jit(solution)/shard_map/all_gather | solution.py:161
  8.5 27.4 %collective-permute-start.3 = (bf16[256,2048]{1,0:T(8,128)(2,1)}, bf16[256,2048]{1,0:T(8,128)(2,1)S(1)}, u32[]{:S(2)}, u32[]{:S(2)}) collective-permute-start(bf16[256,2048]{1,0:T(8,128)(2,1)} %param.19), channel_id=1, source_target_pairs={{0,1},{1,2},{2,3},{3,0},{4,5},{5,6},{6,7},{7,4},{8,9},{9,10},{10,1... | collective-permute-start | bytes 3145736 | tf_op jit(solution)/shard_map/ppermute | solution.py:26
  10.6 33.1 %collective-permute-start.4 = (bf16[256,2048]{1,0:T(8,128)(2,1)}, bf16[256,2048]{1,0:T(8,128)(2,1)}, u32[]{:S(2)}, u32[]{:S(2)}) collective-permute-start(bf16[256,2048]{1,0:T(8,128)(2,1)} %param.19), channel_id=1, source_target_pairs={{0,3},{1,0},{2,1},{3,2},{4,7},{5,4},{6,5},{7,6},{8,11},{9,8},{10,9... | collective-permute-start | bytes 3145736 | tf_op jit(solution)/shard_map/ppermute | solution.py:31
  12.6 19.7 %collective-permute-start.1 = (s32[128]{0:T(128)S(1)}, s32[128]{0:T(128)S(1)}, u32[]{:S(2)}, u32[]{:S(2)}) collective-permute-start(s32[128]{0:T(128)S(1)} %slice.89), channel_id=1, source_target_pairs={{0,4},{4,8},{8,12},{12,16},{16,20},{20,24},{24,28},{28,32},{32,36}... | collective-permute-start | bytes 1544 | tf_op jit(solution)/shard_map/ppermute | solution.py:44
  17.8 15.0 %collective-permute-start.2 = (bf16[128,64]{0,1:T(8,128)(2,1)S(1)}, bf16[128,64]{0,1:T(8,128)(2,1)S(1)}, u32[]{:S(2)}, u32[]{:S(2)}) collective-permute-start(bf16[128,64]{0,1:T(8,128)(2,1)S(1)} %slice.92), channel_id=1, source_target_pairs={{0,4},{4,8},{8,12},{12,16},{16,20},{20,24},{24,28},{28,32},{32,36}... | collective-permute-start | bytes 49160 | tf_op jit(solution)/shard_map/ppermute | solution.py:44
  20.4 15.4 %collective-permute-start = (bf16[128,64]{0,1:T(8,128)(2,1)S(1)}, bf16[128,64]{0,1:T(8,128)(2,1)S(1)}, u32[]{:S(2)}, u32[]{:S(2)}) collective-permute-start(bf16[128,64]{0,1:T(8,128)(2,1)S(1)} %slice.87), channel_id=1, source_target_pairs={{0,4},{4,8},{8,12},{12,16},{16,20},{20,24},{24,28},{28,32},{32,36}... | collective-permute-start | bytes 49160 | tf_op jit(solution)/shard_map/ppermute | solution.py:44
  25.7 7.1 %copy-start.1 = (bf16[1024,64]{0,1:T(8,128)(2,1)S(1)}, bf16[1024,64]{0,1:T(8,128)(2,1)}, u32[]{:S(2)}) copy-start(bf16[1024,64]{0,1:T(8,128)(2,1)} %param.14) | copy-start | bytes 393220
  30.3 4.4 %copy-start.7 = (f32[4]{0:T(128)S(1)}, f32[4]{0:T(128)}, u32[]{:S(2)}) copy-start(f32[4]{0:T(128)} %param.17) | copy-start | bytes 52
  32.8 3.1 %copy-start.2 = (bf16[1024,64]{0,1:T(8,128)(2,1)S(1)}, bf16[1024,64]{0,1:T(8,128)(2,1)}, u32[]{:S(2)}) copy-start(bf16[1024,64]{0,1:T(8,128)(2,1)} %param.15) | copy-start | bytes 393220
  35.9 25.9 %collective-permute-start.5 = (bf16[256,2048]{1,0:T(8,128)(2,1)S(1)}, bf16[256,2048]{1,0:T(8,128)(2,1)S(1)}, u32[]{:S(2)}, u32[]{:S(2)}) collective-permute-start(bf16[256,2048]{1,0:T(8,128)(2,1)S(1)} %collective-permute-done.3), channel_id=1, source_target_pairs={{0,1},{1,2},{2,3},{3,0},{4,5},{5,6},{6,7},{7,4},{8,9},{9,10},{10,1... | collective-permute-start | bytes 3145736 | tf_op jit(solution)/shard_map/ppermute | solution.py:26
  38.8 28.1 %all-to-all-start = ((bf16[4,256,256]{1,2,0:T(8,128)(2,1)}), bf16[4,256,256]{1,2,0:T(8,128)(2,1)S(1)}, u32[]{:S(2)}, u32[]{:S(2)}) async-start(bf16[4,256,256]{1,2,0:T(8,128)(2,1)} %copy.33), calls=%async_computation | async-start | bytes 1048576 | tf_op jit(solution)/shard_map/all_to_all | solution.py:139
  62.9 8.9 %copy-start.6 = (f32[2048]{0:T(1024)S(1)}, f32[2048]{0:T(1024)}, u32[]{:S(2)}) copy-start(f32[2048]{0:T(1024)} %param.20) | copy-start | bytes 24580
  66.9 0.8 copy-start.3
  74.6 5.3 %copy-start.4 = (f32[3,1408]{1,0:T(4,128)S(1)}, f32[3,1408]{1,0:T(4,128)}, u32[]{:S(2)}) copy-start(f32[3,1408]{1,0:T(4,128)} %param.24) | copy-start | bytes 50692
  74.6 5.3 %copy-start.5 = (f32[3,1408]{1,0:T(4,128)S(1)}, f32[3,1408]{1,0:T(4,128)}, u32[]{:S(2)}) copy-start(f32[3,1408]{1,0:T(4,128)} %param.23) | copy-start | bytes 50692
  74.6 52.4 %all-to-all-start.1 = ((bf16[4,256,2048]{2,1,0:T(8,128)(2,1)}), bf16[4,256,2048]{2,1,0:T(8,128)(2,1)}, u32[]{:S(2)}, u32[]{:S(2)}) async-start(bf16[4,256,2048]{2,1,0:T(8,128)(2,1)} %broadcast_in_dim.63), calls=%async_computation.1 | async-start | bytes 8388608 | tf_op jit(solution)/shard_map/all_to_all | solution.py:55
  79.7 148.7 %reduce-scatter.2.cloned.1.call-start = ((), (), s32[]{:S(2)}) async-start(), calls=%async_computation.5 | async-start | bytes 5242880 | tf_op jit(solution)/shard_map/reduce_scatter | solution.py:163
  127.0 15.3 %copy-start.8 = (bf16[2048,2816]{1,0:T(8,128)(2,1)S(1)}, bf16[2048,2816]{1,0:T(8,128)(2,1)}, u32[]{:S(2)}) copy-start(bf16[2048,2816]{1,0:T(8,128)(2,1)} %all-gather.3.cloned.1.call-done) | copy-start | bytes 34603012
  137.3 15.5 %collective-permute-start.6 = (bf16[2,1408]{1,0:T(2,128)(2,1)S(1)}, bf16[2,1408]{1,0:T(2,128)(2,1)S(1)}, u32[]{:S(2)}, u32[]{:S(2)}) collective-permute-start(bf16[2,1408]{1,0:T(2,128)(2,1)S(1)} %slice.114), channel_id=1, source_target_pairs={{0,4},{4,8},{8,12},{12,16},{16,20},{20,24},{24,28},{28,32},{32,36}... | collective-permute-start | bytes 16904 | tf_op jit(solution)/shard_map/ppermute | solution.py:44
  150.9 5.0 %collective-permute-start.7 = (bf16[2,1408]{1,0:T(2,128)(2,1)S(1)}, bf16[2,1408]{1,0:T(2,128)(2,1)S(1)}, u32[]{:S(2)}, u32[]{:S(2)}) collective-permute-start(bf16[2,1408]{1,0:T(2,128)(2,1)S(1)} %slice.121), channel_id=1, source_target_pairs={{0,4},{4,8},{8,12},{12,16},{16,20},{20,24},{24,28},{28,32},{32,36}... | collective-permute-start | bytes 16904 | tf_op jit(solution)/shard_map/ppermute | solution.py:44
Sparse Core Ops, SparseCore 0:
  9.6 63.9 all-gather.2
  75.8 47.7 all-gather.4
  181.3 47.0 reduce-scatter.1
